TPU v7x, 32 devices: a whole 2x2x4 slice. The times are simulated.
32 devices in a mesh: ep: 8 (over z, x), tp: 4 (over y, core).
Axes of the slice: x: 2, y: 2, z: 4, core: 2. Of those that a mesh axis runs over, the one named last changes fastest.
Arguments:
- queries: bfloat16 [2048, 1024], P('ep', 'tp'), may hold values from -256 to 256
- key_rows: bfloat16 [2048, 1024], P('ep', 'tp'), may hold values from -8 to 8
- value_rows: bfloat16 [2048, 1024], P('ep', 'tp'), may hold values from -6 to 6
- head_lambda: float32 [8], P('tp'), may hold values from 0.3 to 0.8
- sub_gain: float32 [128], replicated, may hold values from 0.1 to 1.9
- out_weight: bfloat16 [1024, 2048], P('tp'), may hold values from -0.1875 to 0.1875
- expert_input: bfloat16 [1536, 2048], P('ep'), may hold values from -6 to 6
- norm_gain: float32 [2048], replicated, may hold values from 0.1 to 1.9
- route_ids: int32 [1536, 2], P('ep'), may hold values from 0 to 7, all different within a row; in each aligned block of 192 rows (0 to 191, 192 to 383, ...) at most 80 rows name the same one
- route_weight: float32 [1536, 2], P('ep'), may hold values from 0.25 to 1
- gate_weight: bfloat16 [8, 2048, 3584], P('ep', None, 'tp'), may hold values from -0.125 to 0.125
- up_weight: bfloat16 [8, 2048, 3584], P('ep', None, 'tp'), may hold values from -0.125 to 0.125
- down_weight: bfloat16 [8, 3584, 2048], P('ep', 'tp'), may hold values from -0.09375 to 0.09375
Outputs:
- mixer_out: bfloat16 [2048, 2048], P(('ep', 'tp'))
- expert_out: bfloat16 [1536, 2048], P('ep', 'tp')
Inputs may be any that keep to these rules, and one draw needn't show every extreme that they name: `route_ids`: each row names 2 different experts. In each aligned block of 192 rows no expert is named by more than 80 rows, a bound that some block reaches.
All inputs are finite; a program needn't handle non-finite values.
Results may differ from a plain program's by a relative error of at most 0.014.
Values may be sent and summed in bfloat16 or wider, within the bound.
A program may use at most 256 MiB of HBM per device.

v0:
```python
import functools

import jax
import jax.numpy as jnp
from jax import lax
from jax.experimental import pallas as pl
from jax.experimental.pallas import tpu as pltpu
from jax.sharding import PartitionSpec as P

EPS = 1e-06
MESH = pl.DeviceIdType.MESH
F32 = jnp.float32
BF16 = jnp.bfloat16


def flip(index, bits):
    low = 1
    while low <= bits:
        if bits & low:
            index = index + low - 2 * low * ((index // low) % 2)
        low *= 2
    return index


def dot(a, b, dims=((1,), (0,)), precision=None):
    return lax.dot_general(a, b, (dims, ((), ())), precision=precision, preferred_element_type=F32)


def kernel(
    n_ep, cap, lam, q, k, v, gain, x, norm_gain, ids, route_w, wo_hbm, wg_hbm, wu_hbm, wd_hbm,
    mixer, expert,
    wo, wg, wu, wd, arr, hidden, part, sib, ysend, yrecv, res, ret, kbuf, vbuf,
    outb, qs, comb, acc, top, att, hp, hsib, hysend, hyrecv,
    w_sem, d_send, d_recv, f_send, f_recv, r_send, r_recv, s_send, s_recv, y_send, y_recv,
    kv_send, kv_recv, h_send, h_recv,
):
    me = lax.axis_index("ep")
    tp = lax.axis_index("tp")
    half = n_ep // 2
    tokens, width = x.shape
    cols = width // 4
    units = wg.shape[1]
    core = tp % 2
    sib_tp, y_tp = flip(tp, 1), flip(tp, 2)

    def remote(src, dst, ssem, rsem, where):
        return pltpu.make_async_remote_copy(
            src_ref=src, dst_ref=dst, send_sem=ssem, recv_sem=rsem,
            device_id=where, device_id_type=MESH,
        )

    weights = [
        pltpu.make_async_copy(a, b, w_sem.at[i])
        for i, (a, b) in enumerate(((wg_hbm, wg), (wu_hbm, wu), (wd_hbm, wd), (wo_hbm, wo)))
    ]
    for copy in weights:
        copy.start()

    barrier = pltpu.get_barrier_semaphore()
    for d in range(1, n_ep):
        pl.semaphore_signal(barrier, inc=1, device_id=(flip(me, d), tp), device_id_type=MESH)
    for d in range(1, 4):
        pl.semaphore_signal(barrier, inc=1, device_id=(me, flip(tp, d)), device_id_type=MESH)

    lane = lax.broadcasted_iota(jnp.int32, (tokens, 128), 1)
    id0, id1 = ids[:, 0:1], ids[:, 1:2]
    hot0, hot1 = (lane == id0).astype(F32), (lane == id1).astype(F32)
    earlier = (
        lax.broadcasted_iota(jnp.int32, (tokens, tokens), 1)
        < lax.broadcasted_iota(jnp.int32, (tokens, tokens), 0)
    ).astype(F32).astype(BF16)
    rank = dot(earlier, (hot0 + hot1).astype(BF16))
    pos0 = (id0 * cap).astype(F32) + jnp.sum(rank * hot0, axis=1, keepdims=True)
    pos1 = (id1 * cap).astype(F32) + jnp.sum(rank * hot1, axis=1, keepdims=True)
    packed = jnp.where(lane == 0, pos0, jnp.where(lane == 1, pos1, 0.0))
    pick = (
        lax.broadcasted_iota(jnp.int32, (8, 128), 0) == lax.broadcasted_iota(jnp.int32, (8, 128), 1)
    ).astype(F32)
    pos_rows = dot(pick, packed, ((1,), (1,)), lax.Precision.HIGHEST)
    row0 = (pos_rows[0:1] + 0.5).astype(jnp.int32)
    row1 = (pos_rows[1:2] + 0.5).astype(jnp.int32)
    slots = n_ep * cap
    slot = lax.broadcasted_iota(jnp.int32, (slots, tokens), 0)
    dispatch = ((slot == row0) | (slot == row1)).astype(F32).astype(BF16)
    wide = x[...].astype(F32)
    inv = lax.rsqrt(jnp.mean(wide * wide, axis=-1, keepdims=True) + EPS)
    mine = pl.ds(pl.multiple_of(tp * cols, cols), cols)
    normed = (x[:, mine].astype(F32) * inv * norm_gain[:, mine]).astype(BF16)
    outb[...] = dot(dispatch, normed).astype(BF16).reshape(n_ep, cap, cols)
    slot_c = lax.broadcasted_iota(jnp.int32, (tokens, slots), 1)
    comb[...] = jnp.where(slot_c == pos0.astype(jnp.int32), route_w[:, 0:1], 0.0) + jnp.where(
        slot_c == pos1.astype(jnp.int32), route_w[:, 1:2], 0.0
    )
    arr[tp, me] = outb[me]
    kbuf[me] = k[...]
    vbuf[me] = v[...]
    pl.semaphore_wait(barrier, n_ep - 1 + 3)

    sends = {}
    for d in range(1, n_ep):
        to = flip(me, d)
        sends[d] = remote(
            outb.at[to], arr.at[tp, me], d_send.at[d], d_recv.at[d], (to, tp)
        )
        sends[d].start()

    pending = [[], []]
    relays = [[], []]

    def forward(group):
        for d in range(group * half, (group + 1) * half):
            src = flip(me, d)
            if d:
                sends[d].wait_recv()
            for j, to in ((0, sib_tp), (1, y_tp)):
                c = remote(arr.at[tp, src], arr.at[tp, src], f_send.at[j, d], f_recv.at[j, d], (me, to))
                c.start()
                pending[group].append((j, c))

    def relay(group):
        first = [c for j, c in pending[group] if j == 1]
        for i, d in enumerate(range(group * half, (group + 1) * half)):
            first[i].wait_recv()
            src = flip(me, d)
            c = remote(
                arr.at[y_tp, src], arr.at[y_tp, src], f_send.at[2, d], f_recv.at[2, d], (me, sib_tp)
            )
            c.start()
            relays[group].append(c)

    def arrived(group):
        for j, c in pending[group]:
            if j == 0:
                c.wait_recv()
        for c in relays[group]:
            c.wait_recv()

    mine_half = me // half
    rows = half * cap

    def base_of(group):
        return (mine_half + group * (1 - 2 * mine_half)) * half

    def gate_up(group):
        base = base_of(group)

        def step(i, carry):
            at = pl.ds(pl.multiple_of(i * 128, 128), 128)
            total = jnp.zeros((rows, 256), F32)
            for t in range(4):
                w = jnp.concatenate(
                    [wg[t * cols:(t + 1) * cols, at], wu[t * cols:(t + 1) * cols, at]], axis=1
                )
                total += dot(arr[t, pl.ds(base, half)].reshape(rows, cols), w)
            g, u = total[:, :128], total[:, 128:]
            hidden[:, at] = (g / (1.0 + jnp.exp(-g)) * u).astype(BF16)
            return carry

        lax.fori_loop(0, units // 128, step, 0)

    def down(group):
        base = base_of(group)
        for t in range(4):
            def step(i, carry):
                at = pl.multiple_of(i * 256, 256)
                out = dot(hidden[...], wd[:, pl.ds(t * cols + at, 256)])
                part[t, pl.ds(base, half), :, pl.ds(at, 256)] = out.astype(BF16).reshape(half, cap, 256)
                return carry

            lax.fori_loop(0, cols // 256, step, 0)

    def pair_sum(group):
        base = base_of(group)
        copies = []
        for y in range(2):
            c = remote(
                part.at[2 * y + 1 - core, pl.ds(base, half)], sib.at[y, pl.ds(base, half)],
                s_send.at[group, y], s_recv.at[group, y], (me, sib_tp),
            )
            c.start()
            copies.append(c)
        return copies

    my_y = tp // 2

    def y_sum(group, copies):
        base = base_of(group)
        at = pl.ds(base, half)
        for c in copies:
            c.wait()
        ysend[at] = (part[y_tp, at].astype(F32) + sib[1 - my_y, at].astype(F32)).astype(BF16)
        c = remote(ysend.at[at], yrecv.at[at], y_send.at[group], y_recv.at[group], (me, y_tp))
        c.start()
        return c

    def give_back(group, copy):
        base = base_of(group)
        at = pl.ds(base, half)
        copy.wait()
        res[at] = (
            part[tp, at].astype(F32) + sib[my_y, at].astype(F32) + yrecv[at].astype(F32)
        ).astype(BF16)
        out = []
        for d in range(group * half, (group + 1) * half):
            if d:
                to = flip(me, d)
                c = remote(res.at[to], ret.at[me], r_send.at[d], r_recv.at[d], (to, tp))
                c.start()
                out.append(c)
            else:
                ret[me] = res[me]
        return out

    across = flip(me, 1)
    level, side = me // 2, me % 2
    levels = n_ep // 2

    def kv_copy(b, way, up):
        buf = kbuf if b == 0 else vbuf
        def make(block):
            to = lax.rem(me + 2, n_ep) if up else across
            idx = block // 2
            return remote(
                buf.at[block], buf.at[block], kv_send.at[way, b, idx], kv_recv.at[way, b, idx], (to, tp)
            )
        return make

    def kv_up(lev):
        block = 2 * lev + side

        @pl.when(level < levels - 1)
        def _():
            for b in range(2):
                kv_copy(b, 0, True)(block).start()

    def kv_over(lev):
        block = 2 * lev + side

        @pl.when((lev < level) | (side == 0))
        def _():
            for b in range(2):
                kv_copy(b, 1, False)(block).start()

    def kv_hop(step):
        @pl.when(level - step >= 0)
        def _():
            lev = level - step
            for b in range(2):
                kv_copy(b, 0, True)(2 * lev + side).wait_recv()
            kv_up(lev)
            kv_over(lev)

    def kv_across(lev):
        block = 2 * lev + 1 - side
        for b in range(2):
            kv_copy(b, 1, False)(block).wait_recv()

    def kv_finish():
        def step(lev, carry):
            block = 2 * lev + side

            @pl.when(level < levels - 1)
            def _():
                for b in range(2):
                    kv_copy(b, 0, True)(block).wait_send()

            @pl.when((lev < level) | (side == 0))
            def _():
                for b in range(2):
                    kv_copy(b, 1, False)(block).wait_send()

            return carry

        lax.fori_loop(0, level + 1, step, 0)

    q_rows = q.shape[0]
    heads = lam.shape[0]
    pair = q.shape[1] // heads
    head_width = pair // 2
    head_lane = lax.broadcasted_iota(jnp.int32, (q_rows, pair), 1)

    def attend_own():
        for h in range(heads):
            at = slice(h * pair, (h + 1) * pair)
            qh = q[:, at].astype(F32) * (head_width ** -0.5)
            qs[h, :q_rows] = jnp.where(head_lane < head_width, qh, 0.0).astype(BF16)
            qs[h, q_rows:] = jnp.where(head_lane < head_width, 0.0, qh).astype(BF16)
            s = dot(qs[h], k[:, at], ((1,), (1,)))
            qp = lax.broadcasted_iota(jnp.int32, s.shape, 0) % q_rows
            ok = qp >= lax.broadcasted_iota(jnp.int32, s.shape, 1)
            s = jnp.where(ok, s, -1e30)
            m = jnp.max(s, axis=1, keepdims=True)
            w = jnp.where(ok, jnp.exp(s - m), 0.0)
            top[h] = m
            acc[h] = dot(w.astype(BF16), with_ones(v[:, at]))

    def with_ones(vb):
        return jnp.concatenate([vb, jnp.ones(vb.shape, BF16)], axis=1)

    def attend(first, count):
        span = pl.ds(first, count)
        for h in range(heads):
            at = slice(h * pair, (h + 1) * pair)
            kb = kbuf[span, :, at].reshape(count * q_rows, pair)
            vb = vbuf[span, :, at].reshape(count * q_rows, pair)
            s = dot(qs[h], kb, ((1,), (1,)))
            old = top[h]
            m = jnp.maximum(old, jnp.max(s, axis=1, keepdims=True))
            w = jnp.exp(s - m)
            top[h] = m
            acc[h] = acc[h] * jnp.exp(old - m) + dot(w.astype(BF16), with_ones(vb))

    def attend_level():
        @pl.when(side == 1)
        def _():
            kv_across(level)
            attend(2 * level, 1)

    def attend_rest(lo, hi):
        def step(i, carry):
            kv_across(level - i)
            attend(2 * (level - i), 2)
            return carry

        lax.fori_loop(lo, jnp.minimum(hi, level + 1), step, 0)

    def project():
        outs = []
        for h in range(heads):
            a = acc[h, :, :pair] / acc[h, :, pair:]
            contrast = a[:q_rows] - lam[h] * a[q_rows:]
            norm = lax.rsqrt(jnp.mean(contrast * contrast, axis=-1, keepdims=True) + EPS)
            outs.append((contrast * norm * gain[...]).astype(BF16))
        att[...] = jnp.concatenate(outs, axis=1)

        def step(i, carry):
            at = pl.ds(pl.multiple_of(i * 256, 256), 256)
            hp[:, :, at] = dot(att[...], wo[:, at]).astype(BF16).reshape(4, q_rows // 4, 256)
            return carry

        lax.fori_loop(0, width // 256, step, 0)
        copies = []
        for y in range(2):
            c = remote(
                hp.at[2 * y + 1 - core], hsib.at[y], h_send.at[y], h_recv.at[y], (me, sib_tp)
            )
            c.start()
            copies.append(c)
        return copies

    kv_over(level)
    attend_own()
    forward(0)
    relay(0)
    forward(1)
    kv_up(level)
    weights[0].wait()
    weights[1].wait()
    arrived(0)
    gate_up(0)
    relay(1)
    weights[2].wait()
    down(0)
    pair0 = pair_sum(0)
    kv_hop(1)
    arrived(1)
    gate_up(1)
    y0 = y_sum(0, pair0)
    for step in range(2, min(levels, 3)):
        kv_hop(step)
    down(1)
    pair1 = pair_sum(1)
    for step in range(3, levels):
        kv_hop(step)
    back = give_back(0, y0)
    attend_level()
    y1 = y_sum(1, pair1)
    attend_rest(1, 2)
    back += give_back(1, y1)
    attend_rest(2, levels)
    weights[3].wait()
    hcopies = project()
    for c in hcopies:
        c.wait()
    hysend[...] = (hp[y_tp].astype(F32) + hsib[1 - my_y].astype(F32)).astype(BF16)
    hy = remote(hysend, hyrecv, h_send.at[2], h_recv.at[2], (me, y_tp))
    hy.start()
    for d in range(1, n_ep):
        sends[d].wait_send()
    for group in range(2):
        for j, c in pending[group]:
            c.wait_send()
        for c in relays[group]:
            c.wait_send()
    kv_finish()
    hy.wait()
    mixer[...] = (hp[tp].astype(F32) + hsib[my_y].astype(F32) + hyrecv[...].astype(F32)).astype(BF16)
    for c in back:
        c.wait()
    big = comb[...]
    high = big.astype(BF16)
    low = (big - high.astype(F32)).astype(BF16)
    got = ret[...].reshape(slots, cols)
    expert[...] = (dot(high, got) + dot(low, got)).astype(BF16)


def solution(mesh):
    n_ep = mesh.shape["ep"]

    def shards(
        queries, key_rows, value_rows, head_lambda, sub_gain, out_weight, expert_input, norm_gain,
        route_ids, route_weight, gate_weight, up_weight, down_weight,
    ):
        tokens, width = expert_input.shape
        cap = 5 * route_ids.shape[1] * tokens // (3 * n_ep)
        cap = -(-cap // 16) * 16
        cols = width // 4
        half = n_ep // 2
        units = gate_weight.shape[2]
        q_rows, kv_cols = queries.shape
        heads = head_lambda.shape[0]
        vm = pl.BlockSpec(memory_space=pltpu.VMEM)
        hbm = pl.BlockSpec(memory_space=pl.ANY)
        dma = pltpu.SemaphoreType.DMA
        return pl.pallas_call(
            functools.partial(kernel, n_ep, cap),
            name="both_halves",
            out_shape=(
                jax.ShapeDtypeStruct((q_rows // 4, width), BF16),
                jax.ShapeDtypeStruct((tokens, cols), BF16),
            ),
            in_specs=[pl.BlockSpec(memory_space=pltpu.SMEM)] + [vm] * 8 + [hbm] * 4,
            out_specs=(vm, vm),
            scratch_shapes=[
                pltpu.VMEM(out_weight.shape, BF16),
                pltpu.VMEM((width, units), BF16),
                pltpu.VMEM((width, units), BF16),
                pltpu.VMEM((units, width), BF16),
                pltpu.VMEM((4, n_ep, cap, cols), BF16),
                pltpu.VMEM((half * cap, units), BF16),
                pltpu.VMEM((4, n_ep, cap, cols), BF16),
                pltpu.VMEM((2, n_ep, cap, cols), BF16),
                pltpu.VMEM((n_ep, cap, cols), BF16),
                pltpu.VMEM((n_ep, cap, cols), BF16),
                pltpu.VMEM((n_ep, cap, cols), BF16),
                pltpu.VMEM((n_ep, cap, cols), BF16),
                pltpu.VMEM((n_ep, q_rows, kv_cols), BF16),
                pltpu.VMEM((n_ep, q_rows, kv_cols), BF16),
                pltpu.VMEM((n_ep, cap, cols), BF16),
                pltpu.VMEM((heads, 2 * q_rows, 128), BF16),
                pltpu.VMEM((tokens, n_ep * cap), F32),
                pltpu.VMEM((heads, 2 * q_rows, 2 * kv_cols // heads), F32),
                pltpu.VMEM((heads, 2 * q_rows, 1), F32),
                pltpu.VMEM((q_rows, kv_cols), BF16),
                pltpu.VMEM((4, q_rows // 4, width), BF16),
                pltpu.VMEM((2, q_rows // 4, width), BF16),
                pltpu.VMEM((q_rows // 4, width), BF16),
                pltpu.VMEM((q_rows // 4, width), BF16),
                dma((4,)),
                dma((n_ep,)), dma((n_ep,)),
                dma((3, n_ep)), dma((3, n_ep)),
                dma((n_ep,)), dma((n_ep,)),
                dma((2, 2)), dma((2, 2)),
                dma((2,)), dma((2,)),
                dma((2, 2, half)), dma((2, 2, half)),
                dma((3,)), dma((3,)),
            ],
            compiler_params=pltpu.CompilerParams(
                collective_id=0, has_side_effects=True, vmem_limit_bytes=62 * 1024 * 1024
            ),
        )(
            head_lambda, queries, key_rows, value_rows, sub_gain.reshape(1, -1), expert_input,
            norm_gain.reshape(1, -1), route_ids, route_weight, out_weight,
            gate_weight[0], up_weight[0], down_weight[0],
        )

    placed = (
        P("ep", "tp"), P("ep", "tp"), P("ep", "tp"), P("tp"), P(), P("tp", None), P("ep", None), P(),
        P("ep", None), P("ep", None), P("ep", None, "tp"), P("ep", None, "tp"), P("ep", "tp", None),
    )
    return jax.shard_map(
        shards, mesh=mesh, in_specs=placed,
        out_specs=(P(("ep", "tp"), None), P("ep", "tp")), check_vma=False,
    )
```

profile of v0, /device:TPU:0, one launch (start us, length us, event | category | flops | bytes accessed | tf_op | source)
XLA Modules:
  0.0 71.6 jit_solution(10306454347401243258)
XLA Ops:
  0.6 1.4 %copy.15.ids = s32[192,2]{1,0:T(8,128)} copy(s32[192,2]{0,1:T(2,128)} %param.21) | data formatting | bytes 3072 | tf_op args[8]
  2.1 1.4 %copy.16.route_w = f32[192,2]{1,0:T(8,128)} copy(f32[192,2]{0,1:T(2,128)} %param.22) | data formatting | bytes 3072 | tf_op args[9]
  3.5 64.8 %both_halves.1 = (bf16[64,2048]{1,0:T(8,128)(2,1)}, bf16[192,512]{1,0:T(8,128)(2,1)}) custom-call(f32[2]{0:T(128)} %lam.1, bf16[256,256]{1,0:T(8,128)(2,1)} %q.1, bf16[256,256]{1,0:T(8,128)(2,1)} %k.1, bf16[256,256]{1,0:T(8,128)(2,1)} %v.1, f32[1,128]{1,0:T(1,128)} %bitcast.9, bf16[192,2048]{1,0:T(8,128)(2,1)} %x.1, f32[1,2048]{1,0:T(1,128)} %bitcast.8, ...), custom_call_target="tpu_custom_call" | custom-call | tf_op jit(solution)/shard_map/both_halves/pallas_call | solution.py:425
  68.3 1.7 %copy.19 = bf16[64,2048]{1,0:T(8,128)(2,1)} copy(bf16[64,2048]{1,0:T(8,128)(2,1)} %get-tuple-element.4) | data formatting | bytes 524288
  69.9 1.6 %copy.20 = bf16[192,512]{1,0:T(8,128)(2,1)} copy(bf16[192,512]{1,0:T(8,128)(2,1)} %get-tuple-element.5) | data formatting | bytes 393216
where the time goes:
time: 72.3 us; the launch traced here: 71.6 us
  Pallas kernels  64.8 us (90%)
  local copies, waits for them, and re-layouts  6.17 us (9%)
    pallas_call x1, Pallas kernels, shards(): pl.pallas_call(functools.partial(kernel, n_ep, cap), name='both_halves',...  64.8 us
    unnamed x4, local copies, waits for them, and re-layouts  6.17 us

commit v1 on v0

v1 whole, which is shorter than its diff:
```python
import functools

import jax
import jax.numpy as jnp
from jax import lax
from jax.experimental import pallas as pl
from jax.experimental.pallas import tpu as pltpu
from jax.sharding import PartitionSpec as P

EPS = 1e-06
MESH = pl.DeviceIdType.MESH
F32 = jnp.float32
BF16 = jnp.bfloat16


def flip(index, bits):
    low = 1
    while low <= bits:
        if bits & low:
            index = index + low - 2 * low * ((index // low) % 2)
        low *= 2
    return index


def dot(a, b, dims=((1,), (0,)), precision=None):
    return lax.dot_general(a, b, (dims, ((), ())), precision=precision, preferred_element_type=F32)


def kernel(
    n_ep, cap, lam, q, k, v, gain, x, norm_gain, ids, route_w, wo_hbm, wg_hbm, wu_hbm, wd_hbm,
    mixer, expert,
    wo, wg, wu, wd, arr, hidden, part, sib, ysend, yrecv, res, ret, kbuf, vbuf,
    outb, nrm, info, nrm_in, info_in, spread, qx, qs, high, low, acc, top, mix, att, hp, hsib, hysend, hyrecv,
    w_sem, d_send, d_recv, f_send, f_recv, r_send, r_recv, s_send, s_recv, y_send, y_recv,
    g_send, g_recv, x_send, x_recv, kv_send, kv_recv, k2_send, h_send, h_recv,
):
    me = lax.axis_index("ep")
    tp = lax.axis_index("tp")
    half, quarter = n_ep // 2, n_ep // 4
    upper = me // half
    near = (upper * half, half)
    inner = (half - upper * quarter, quarter)
    outer = ((1 - upper) * (half + quarter), quarter)
    mate = flip(me, half + quarter)
    first = upper * half
    tokens, width = x.shape
    cols = width // 4
    units = wg.shape[1]
    sib_tp, y_tp = flip(tp, 1), flip(tp, 2)

    def remote(src, dst, ssem, rsem, where):
        return pltpu.make_async_remote_copy(
            src_ref=src, dst_ref=dst, send_sem=ssem, recv_sem=rsem,
            device_id=where, device_id_type=MESH,
        )

    weights = [
        pltpu.make_async_copy(a, b, w_sem.at[i])
        for i, (a, b) in enumerate(((wg_hbm, wg), (wu_hbm, wu), (wd_hbm, wd), (wo_hbm, wo)))
    ]
    for copy in weights:
        copy.start()

    barrier = pltpu.get_barrier_semaphore()
    for d in range(1, n_ep):
        pl.semaphore_signal(barrier, inc=1, device_id=(flip(me, d), tp), device_id_type=MESH)
    for d in range(1, 4):
        pl.semaphore_signal(barrier, inc=1, device_id=(me, flip(tp, d)), device_id_type=MESH)

    slots = n_ep * cap
    id0, id1 = ids[0:1, :], ids[1:2, :]
    index = lax.broadcasted_iota(jnp.int32, (max(n_ep, 8), tokens), 0)
    hot0, hot1 = (index == id0).astype(F32), (index == id1).astype(F32)
    earlier = (
        lax.broadcasted_iota(jnp.int32, (tokens, tokens), 0)
        < lax.broadcasted_iota(jnp.int32, (tokens, tokens), 1)
    ).astype(F32).astype(BF16)
    rank = dot((hot0 + hot1).astype(BF16), earlier)
    row0 = id0 * cap + (jnp.sum(rank * hot0, axis=0, keepdims=True) + 0.5).astype(jnp.int32)
    row1 = id1 * cap + (jnp.sum(rank * hot1, axis=0, keepdims=True) + 0.5).astype(jnp.int32)
    slot = lax.broadcasted_iota(jnp.int32, (slots, tokens), 0)
    here = lax.broadcasted_iota(jnp.int32, (half * cap, tokens), 0) + first * cap
    dispatch = ((here == row0) | (here == row1)).astype(F32).astype(BF16)
    wide = x[...].astype(F32)
    inv = lax.rsqrt(jnp.mean(wide * wide, axis=-1, keepdims=True) + EPS)
    mine = pl.ds(pl.multiple_of(tp * cols, cols), cols)
    normed = (x[:, mine].astype(F32) * inv * norm_gain[:, mine]).astype(BF16)
    nrm[...] = normed
    line = lax.broadcasted_iota(jnp.int32, (8, tokens), 0)
    info[...] = jnp.where(line == 0, row0, jnp.where(line == 1, row1, 0)).astype(F32)
    outb[...] = dot(dispatch, normed).astype(BF16).reshape(half, cap, cols)
    pl.semaphore_wait(barrier, n_ep - 1 + 3)

    def dispatch_to(at):
        return remote(outb.at[at - first], arr.at[tp, me], d_send.at[at], d_recv.at[me], (at, tp))

    def spread_to(at):
        return remote(
            spread.at[at - first], arr.at[tp, mate], d_send.at[flip(at, half)], d_recv.at[mate], (at, tp)
        )

    def dispatch_from(at):
        return remote(outb.at[0], arr.at[tp, at], d_send.at[at], d_recv.at[at], (at, tp))

    def to_mate(i):
        src, dst = ((info, info_in), (nrm, nrm_in))[i]
        return remote(src, dst, g_send.at[i], g_recv.at[i], (mate, tp))

    def sources(group):
        base, size = group
        return [flip(base + me % size, i) for i in range(size)]

    def others(group):
        return sources(group)[1:] if group is near else sources(group)

    def send(ds):
        for d in ds:
            dispatch_to(flip(me, d)).start()

    def send_mate():
        to_mate(0).start()
        to_mate(1).start()

    at_middle = (me // quarter == 1) | (me // quarter == 2)

    def expand(condition):
        @pl.when(condition)
        def _():
            to_mate(0).wait_recv()
            to_mate(1).wait_recv()
            place = here.astype(F32)
            pick = ((place == info_in[0:1]) | (place == info_in[1:2])).astype(F32).astype(BF16)
            spread[...] = dot(pick, nrm_in[...]).astype(BF16).reshape(half, cap, cols)
            for at in others(near):
                spread_to(at).start()
            arr[tp, mate] = spread[me - first]

    def own_rows():
        local = lax.broadcasted_iota(jnp.int32, (cap, tokens), 0) + me * cap
        pick = ((local == row0) | (local == row1)).astype(F32).astype(BF16)
        for t in range(4):
            at = slice(t * cols, (t + 1) * cols)
            rows = (x[:, at].astype(F32) * inv * norm_gain[:, at]).astype(BF16)
            arr[t, me] = dot(pick, rows).astype(BF16)

    def weigh():
        comb = jnp.where(slot == row0, route_w[0:1, :], 0.0) + jnp.where(
            slot == row1, route_w[1:2, :], 0.0
        )
        big = comb.astype(BF16).astype(F32)
        high[...] = comb.T.astype(BF16)
        low[...] = (comb - big).T.astype(BF16)

    def to_sib(src):
        return remote(
            arr.at[tp, src], arr.at[tp, src], f_send.at[0, src], f_recv.at[0, src], (me, sib_tp)
        )

    def to_y(src):
        return remote(
            arr.at[tp, src], arr.at[tp, src], f_send.at[1, src], f_recv.at[1, src], (me, y_tp)
        )

    def y_to_sib(src):
        return remote(
            arr.at[y_tp, src], arr.at[y_tp, src], f_send.at[2, src], f_recv.at[2, src], (me, sib_tp)
        )

    def forward(src):
        @pl.when(src != mate)
        def _():
            dispatch_from(src).wait_recv()

        to_y(src).start()
        to_sib(src).start()

    def relay(src):
        to_y(src).wait_recv()
        y_to_sib(src).start()

    def arrived(src):
        to_sib(src).wait_recv()
        y_to_sib(src).wait_recv()

    def gate_up(group, lo, hi):
        base, rows = group[0], group[1] * cap
        got = [arr[t, pl.ds(base, group[1])].reshape(rows, cols) for t in range(4)]
        for lo in range(lo * 128, min(hi * 128, units), 256):
            n = min(256, units - lo)
            total = jnp.zeros((rows, 2 * n), F32)
            for t in range(4):
                at = slice(t * cols, (t + 1) * cols)
                w = jnp.concatenate([wg[at, lo:lo + n], wu[at, lo:lo + n]], axis=1)
                total += dot(got[t], w)
            g, u = total[:, :n], total[:, n:]
            hidden[:rows, lo:lo + n] = (g / (1.0 + jnp.exp(-g)) * u).astype(BF16)

    def down(group, r):
        base, rows = group[0], group[1] * cap
        at = pl.ds(pl.multiple_of(flip(tp, r) * cols, cols), cols)
        out = dot(hidden[:rows], wd[:, at])
        part[r, pl.ds(base, group[1])] = out.astype(BF16).reshape(group[1], cap, cols)

    pairs = {}

    def pair(group, number, y):
        at = pl.ds(*group)
        c = remote(
            part.at[2 * y + 1, at], sib.at[y, at], s_send.at[number, y], s_recv.at[number, y], (me, sib_tp)
        )
        c.start()
        pairs[number, y] = c

    def over_y(at):
        return remote(ysend.at[at], yrecv.at[at], y_send.at[at], y_recv.at[at], (me, y_tp))

    def y_sum(group, number):
        pairs[number, 1].wait_recv()
        at = pl.ds(*group)
        ysend[at] = (part[2, at].astype(F32) + sib[1, at].astype(F32)).astype(BF16)

    def y_go(srcs):
        for to in srcs:
            over_y(to).start()

    def return_to(at):
        return remote(res.at[at], ret.at[me], r_send.at[at], r_recv.at[me], (at, tp))

    def return_from(at):
        return remote(res.at[at], ret.at[at], r_send.at[at], r_recv.at[at], (at, tp))

    def give_back(to, own=False):
        over_y(to).wait_recv()
        out = (
            part[0, to].astype(F32) + sib[0, to].astype(F32) + yrecv[to].astype(F32)
        ).astype(BF16)
        if own:
            ret[to] = out
        else:
            res[to] = out
            return_to(to).start()

    across = flip(me, 1)
    level, side = me // 2, me % 2
    levels = n_ep // 2
    pinch = levels // 2 - 1

    q_rows = q.shape[0]
    heads = lam.shape[0]
    pair_width = q.shape[1] // heads
    head_width = pair_width // 2
    other = 1 - side
    my_head = pl.ds(pl.multiple_of(side * pair_width, pair_width), pair_width)
    its_head = pl.ds(pl.multiple_of(other * pair_width, pair_width), pair_width)

    def swap(i):
        src, dst = ((k, kbuf.at[level, side]), (v, vbuf.at[level, side]), (q, qx.at[side]))[i]
        return remote(src.at[:, its_head], dst, x_send.at[i], x_recv.at[i], (across, tp))

    def swap_start():
        for i in range(3):
            swap(i).start()
        kbuf[level, side] = k[:, my_head]
        vbuf[level, side] = v[:, my_head]
        qx[side] = q[:, my_head]

    def swap_wait():
        for i in range(3):
            swap(i).wait_recv()

    def kv_copy(b, lev):
        buf = kbuf if b < 2 else vbuf
        at = buf.at[lev, b % 2]
        return remote(at, at, kv_send.at[b, lev], kv_recv.at[b, lev], (lax.rem(me + 2, n_ep), tp))

    def kv_skip(b):
        buf = kbuf if b < 2 else vbuf
        at = buf.at[level, b % 2]
        return remote(at, at, k2_send.at[b], kv_recv.at[b, level], (lax.rem(me + 4, n_ep), tp))

    def kv_first():
        @pl.when(level == pinch - 1)
        def _():
            for b in range(4):
                kv_skip(b).start()

        @pl.when(level < levels - 1)
        def _():
            for b in range(4):
                kv_copy(b, level).start()

    def kv_hop(step):
        for b in range(4):
            kv_copy(b, level - step).wait_recv()
            kv_copy(b, level - step).start()

    def hop_lower():
        for step in range(1, pinch + 1):
            @pl.when((level >= step) & ((level < pinch) | ((level == pinch) & (step > 1))))
            def _():
                kv_hop(step)

    def hop_upper(lo, hi):
        for step in range(lo, hi):
            @pl.when((level > pinch) & (level < levels - 1) & (level >= step))
            def _():
                kv_hop(step)

    def kv_last(step):
        @pl.when(((level == levels - 1) & (level >= step)) | ((level == pinch) & (step == 1)))
        def _():
            for b in range(4):
                kv_copy(b, level - step).wait_recv()

    def kv_finish():
        def step(lev, carry):
            for b in range(4):
                kv_copy(b, lev).wait_send()
            return carry

        @pl.when((level < levels - 1) & (level != pinch))
        def _():
            lax.fori_loop(0, level + 1, step, 0)

        @pl.when(level == pinch)
        def _():
            lax.fori_loop(0, level - 1, step, 0)
            step(level, 0)

        @pl.when(level == pinch - 1)
        def _():
            for b in range(4):
                kv_skip(b).wait_send()

    both = 2 * q_rows
    head_lane = lax.broadcasted_iota(jnp.int32, (both, pair_width), 1)

    def with_ones(vb):
        return jnp.concatenate([vb, jnp.ones(vb.shape, BF16)], axis=1)

    def attend_own():
        qh = qx[...].reshape(both, pair_width).astype(F32) * (head_width ** -0.5)
        kb = kbuf[level].reshape(both, pair_width)
        vb = with_ones(vbuf[level].reshape(both, pair_width))
        for m in range(2):
            first = head_lane < head_width
            qs[m] = jnp.where(first if m == 0 else ~first, qh, 0.0).astype(BF16)
            s = dot(qs[m], kb, ((1,), (1,)))
            ok = lax.broadcasted_iota(jnp.int32, s.shape, 0) >= lax.broadcasted_iota(jnp.int32, s.shape, 1)
            s = jnp.where(ok, s, -1e30)
            t = jnp.max(s, axis=1, keepdims=True)
            w = jnp.exp(s - t)
            top[m] = t
            acc[m] = dot(w.astype(BF16), vb)

    def attend(lev):
        kb = kbuf[lev].reshape(both, pair_width)
        vb = with_ones(vbuf[lev].reshape(both, pair_width))
        for m in range(2):
            s = dot(qs[m], kb, ((1,), (1,)))
            old = top[m]
            t = jnp.maximum(old, jnp.max(s, axis=1, keepdims=True))
            w = jnp.exp(s - t)
            top[m] = t
            acc[m] = acc[m] * jnp.exp(old - t) + dot(w.astype(BF16), vb)

    def attend_at(step):
        @pl.when(level >= step)
        def _():
            attend(level - step)

    def att_swap():
        return remote(mix.at[other], att.at[side], x_send.at[3], x_recv.at[3], (across, tp))

    def normalise():
        a = acc[:, :, :pair_width] / acc[:, :, pair_width:]
        contrast = a[0] - lam[side] * a[1]
        norm = lax.rsqrt(jnp.mean(contrast * contrast, axis=-1, keepdims=True) + EPS)
        mix[...] = (contrast * norm * gain[...]).astype(BF16).reshape(2, q_rows, pair_width)
        att_swap().start()
        att[side] = mix[side]

    def h_pair(y):
        return remote(
            hp.at[flip(tp, 2 * y + 1)], hsib.at[y], h_send.at[y], h_recv.at[y], (me, sib_tp)
        )

    def h_over():
        return remote(hysend, hyrecv, h_send.at[2], h_recv.at[2], (me, y_tp))

    def project():
        att_swap().wait_recv()
        rows = jnp.concatenate([att[h] for h in range(heads)], axis=1)
        hp[...] = dot(rows, wo[...]).astype(BF16).reshape(4, q_rows // 4, width)
        h_pair(1).start()
        h_pair(0).start()

    def h_send_over():
        h_pair(1).wait_recv()
        hysend[...] = (hp[y_tp].astype(F32) + hsib[1].astype(F32)).astype(BF16)
        h_over().start()

    def drain():
        for src in others(near) + sources(inner) + sources(outer):
            to_sib(src).wait_send()
            to_y(src).wait_send()
            y_to_sib(src).wait_send()
            return_to(src).wait_send()
        for src in sources(near) + sources(inner) + sources(outer):
            over_y(src).wait_send()
        for at in others(near):
            dispatch_to(at).wait_send()
            spread_to(at).wait_send()
        for i in range(2):
            to_mate(i).wait_send()
        for c in pairs.values():
            c.wait_send()
        for y in range(2):
            h_pair(y).wait_send()
        for i in range(3):
            swap(i).wait_send()
        att_swap().wait_send()
        kv_finish()

    def mix_out():
        h_pair(0).wait_recv()
        h_over().wait()
        mixer[...] = (
            hp[tp].astype(F32) + hsib[0].astype(F32) + hyrecv[...].astype(F32)
        ).astype(BF16)

    def combine():
        for src in others(near) + sources(inner) + sources(outer):
            return_from(src).wait_recv()
        got = ret[...].reshape(slots, cols)
        expert[...] = (dot(high[...], got) + dot(low[...], got)).astype(BF16)

    send(range(1, half))
    send_mate()
    own_rows()
    weigh()
    forward(others(near)[0])
    swap_start()
    forward(others(near)[1])
    for at in others(near)[2:]: forward(at)
    expand(at_middle)
    relay(others(near)[0])
    swap_wait()
    expand(~at_middle)
    kv_first()
    for at in others(near)[1:]: relay(at)
    for at in sources(inner)[:1]: forward(at)
    for copy in weights[:2]: copy.wait()
    for at in sources(inner)[1:]: forward(at)
    for at in others(near): arrived(at)
    gate_up(near, 0, 4)
    for at in sources(outer)[:1]: forward(at)
    for at in sources(inner)[:1]: relay(at)
    gate_up(near, 4, 7)
    for at in sources(outer)[1:]: forward(at)
    for at in sources(inner)[1:]: relay(at)
    weights[2].wait()
    for r in (3, 1): down(near, r)
    pair(near, 0, 1)
    pair(near, 0, 0)
    for r in (2, 0): down(near, r)
    for at in sources(inner): arrived(at)
    gate_up(inner, 0, 7)
    for at in sources(outer)[:1]: relay(at)
    hop_lower()
    down(inner, 3)
    pair(inner, 1, 1)
    down(inner, 2)
    for at in sources(outer)[1:]: relay(at)
    hop_upper(1, 2)
    down(inner, 1)
    pair(inner, 1, 0)
    down(inner, 0)
    y_sum(inner, 1)
    y_go(sources(inner))
    for at in sources(outer): arrived(at)
    gate_up(outer, 0, 7)
    hop_upper(2, levels)
    down(outer, 3)
    pair(outer, 2, 1)
    down(outer, 2)
    down(outer, 1)
    pair(outer, 2, 0)
    down(outer, 0)
    y_sum(outer, 2)
    y_go(sources(outer))
    y_sum(near, 0)
    y_go(sources(near))
    attend_own()
    pairs[1, 0].wait_recv()
    for at in sources(inner): give_back(at)
    kv_last(1)
    attend_at(1)
    pairs[2, 0].wait_recv()
    for at in sources(outer): give_back(at)
    for step in range(2, levels): kv_last(step); attend_at(step)
    normalise()
    pairs[0, 0].wait_recv()
    for i, at in enumerate(sources(near)): give_back(at, i == 0)
    weights[3].wait()
    project()
    h_send_over()
    combine()
    drain()
    mix_out()


def settle(mixer_in, expert_in, mixer, expert, a, b, load, store):
    pairs = ((mixer_in, a, mixer), (expert_in, b, expert))
    loads = [pltpu.make_async_copy(x, y, load.at[i]) for i, (x, y, _) in enumerate(pairs)]
    stores = [pltpu.make_async_copy(y, z, store.at[i]) for i, (_, y, z) in enumerate(pairs)]
    for copy in loads:
        copy.start()
    for i in range(2):
        loads[i].wait()
        stores[i].start()
    for copy in stores:
        copy.wait()


def solution(mesh):
    n_ep = mesh.shape["ep"]

    def shards(
        queries, key_rows, value_rows, head_lambda, sub_gain, out_weight, expert_input, norm_gain,
        route_ids, route_weight, gate_weight, up_weight, down_weight,
    ):
        tokens, width = expert_input.shape
        cap = 5 * route_ids.shape[1] * tokens // (3 * n_ep)
        cap = -(-cap // 16) * 16
        cols = width // 4
        half = n_ep // 2
        units = gate_weight.shape[2]
        q_rows, kv_cols = queries.shape
        heads = head_lambda.shape[0]
        vm = pl.BlockSpec(memory_space=pltpu.VMEM)
        hbm = pl.BlockSpec(memory_space=pl.ANY)
        dma = pltpu.SemaphoreType.DMA
        outs = pl.pallas_call(
            functools.partial(kernel, n_ep, cap),
            name="both_halves",
            out_shape=(
                jax.ShapeDtypeStruct((q_rows // 4, width), BF16),
                jax.ShapeDtypeStruct((tokens, cols), BF16),
            ),
            in_specs=[pl.BlockSpec(memory_space=pltpu.SMEM)] + [vm] * 8 + [hbm] * 4,
            out_specs=(vm, vm),
            scratch_shapes=[
                pltpu.VMEM(out_weight.shape, BF16),
                pltpu.VMEM((width, units), BF16),
                pltpu.VMEM((width, units), BF16),
                pltpu.VMEM((units, width), BF16),
                pltpu.VMEM((4, n_ep, cap, cols), BF16),
                pltpu.VMEM((half * cap, units), BF16),
                pltpu.VMEM((4, n_ep, cap, cols), BF16),
                pltpu.VMEM((2, n_ep, cap, cols), BF16),
                pltpu.VMEM((n_ep, cap, cols), BF16),
                pltpu.VMEM((n_ep, cap, cols), BF16),
                pltpu.VMEM((n_ep, cap, cols), BF16),
                pltpu.VMEM((n_ep, cap, cols), BF16),
                pltpu.VMEM((half, 2, q_rows, kv_cols // heads), BF16),
                pltpu.VMEM((half, 2, q_rows, kv_cols // heads), BF16),
                pltpu.VMEM((half, cap, cols), BF16),
                pltpu.VMEM((tokens, cols), BF16),
                pltpu.VMEM((8, tokens), F32),
                pltpu.VMEM((tokens, cols), BF16),
                pltpu.VMEM((8, tokens), F32),
                pltpu.VMEM((half, cap, cols), BF16),
                pltpu.VMEM((2, q_rows, kv_cols // heads), BF16),
                pltpu.VMEM((2, 2 * q_rows, kv_cols // heads), BF16),
                pltpu.VMEM((tokens, n_ep * cap), BF16),
                pltpu.VMEM((tokens, n_ep * cap), BF16),
                pltpu.VMEM((2, 2 * q_rows, 2 * kv_cols // heads), F32),
                pltpu.VMEM((2, 2 * q_rows, 1), F32),
                pltpu.VMEM((2, q_rows, kv_cols // heads), BF16),
                pltpu.VMEM((heads, q_rows, kv_cols // heads), BF16),
                pltpu.VMEM((4, q_rows // 4, width), BF16),
                pltpu.VMEM((2, q_rows // 4, width), BF16),
                pltpu.VMEM((q_rows // 4, width), BF16),
                pltpu.VMEM((q_rows // 4, width), BF16),
                dma((4,)),
                dma((n_ep,)), dma((n_ep,)),
                dma((3, n_ep)), dma((3, n_ep)),
                dma((n_ep,)), dma((n_ep,)),
                dma((3, 2)), dma((3, 2)),
                dma((n_ep,)), dma((n_ep,)),
                dma((2,)),dma((2,)),
                dma((4,)), dma((4,)),
                dma((4, half)), dma((4, half)), dma((4,)),
                dma((3,)), dma((3,)),
            ],
            compiler_params=pltpu.CompilerParams(
                collective_id=0, has_side_effects=True, vmem_limit_bytes=62 * 1024 * 1024
            ),
        )(
            head_lambda, queries, key_rows, value_rows, sub_gain.reshape(1, -1), expert_input,
            norm_gain.reshape(1, -1), route_ids.T, route_weight.T, out_weight,
            gate_weight[0], up_weight[0], down_weight[0],
        )
        return pl.pallas_call(
            settle,
            name="settle",
            out_shape=tuple(jax.ShapeDtypeStruct(o.shape, o.dtype) for o in outs),
            in_specs=[hbm] * 2,
            out_specs=(hbm, hbm),
            scratch_shapes=[pltpu.VMEM(o.shape, o.dtype) for o in outs] + [dma((2,)), dma((2,))],
        )(*outs)

    placed = (
        P("ep", "tp"), P("ep", "tp"), P("ep", "tp"), P("tp"), P(), P("tp", None), P("ep", None), P(),
        P("ep", None), P("ep", None), P("ep", None, "tp"), P("ep", None, "tp"), P("ep", "tp", None),
    )
    return jax.shard_map(
        shards, mesh=mesh, in_specs=placed,
        out_specs=(P(("ep", "tp"), None), P("ep", "tp")), check_vma=False,
    )
```

time: 72.3 us -> 62 us (0.86)
  local copies, waits for them, and re-layouts: 6.17 us -> 0 us
  Pallas kernels: 64.8 us -> 61 us
    unnamed x4 -> x0, local copies, waits for them, and re-layouts: 6.17 us -> none
    pallas_call x1, Pallas kernels: 64.8 us -> 59.3 us  [shards(): pl.pallas_call(functools.partial(kernel, n_ep, cap), name='both_halves',...]
    pallas_call x0 -> x1, Pallas kernels: none -> 1.75 us  [shards(): pl.pallas_call(settle, name='settle', out_shape=tuple((jax.ShapeDtypeStru...]
where the time goes in v1:
time: 62 us; the launch traced here: 61.9 us
  Pallas kernels  61 us (98%)
  between operations  0.8 us (1%)
    pallas_call x1, Pallas kernels, shards(): pl.pallas_call(functools.partial(kernel, n_ep, cap), name='both_halves',...  59.3 us
    pallas_call x1, Pallas kernels, shards(): pl.pallas_call(settle, name='settle', out_shape=tuple((jax.ShapeDtypeStru...  1.75 us

profile of v1, /device:TPU:0, one launch (start us, length us, event | category | flops | bytes accessed | tf_op | source)
XLA Modules:
  0.0 61.9 jit_solution(12755815913793209953)
XLA Ops:
  0.6 59.3 %both_halves.1 = (bf16[64,2048]{1,0:T(8,128)(2,1)}, bf16[192,512]{1,0:T(8,128)(2,1)}) custom-call(f32[2]{0:T(128)} %lam.1, bf16[256,256]{1,0:T(8,128)(2,1)} %q.1, bf16[256,256]{1,0:T(8,128)(2,1)} %k.1, bf16[256,256]{1,0:T(8,128)(2,1)} %v.1, f32[1,128]{1,0:T(1,128)} %bitcast.13, bf16[192,2048]{1,0:T(8,128)(2,1)} %x.1, f32[1,2048]{1,0:T(1,128)} %bitcast.10, ...), custom_call_target="tpu_custom_call" | custom-call | tf_op jit(solution)/shard_map/both_halves/pallas_call | solution.py:544
  59.9 1.7 %settle.1 = (bf16[64,2048]{1,0:T(8,128)(2,1)}, bf16[192,512]{1,0:T(8,128)(2,1)}) custom-call(bf16[64,2048]{1,0:T(8,128)(2,1)} %get-tuple-element.4.mixer_in, bf16[192,512]{1,0:T(8,128)(2,1)} %get-tuple-element.5.expert_in), custom_call_target="tpu_custom_call" | custom-call | tf_op jit(solution)/shard_map/settle/pallas_call | solution.py:605

commit v2 on v1

--- a/solution.py
+++ b/solution.py
@@ -39,8 +39,8 @@
     half, quarter = n_ep // 2, n_ep // 4
     upper = me // half
     near = (upper * half, half)
-    inner = (half - upper * quarter, quarter)
-    outer = ((1 - upper) * (half + quarter), quarter)
+    early = ((1 - upper) * half, quarter)
+    late = ((1 - upper) * half + quarter, quarter)
     mate = flip(me, half + quarter)
     first = upper * half
     tokens, width = x.shape
@@ -174,6 +174,12 @@
         to_y(src).start()
         to_sib(src).start()
 
+    def forward_when(condition, srcs):
+        @pl.when(condition)
+        def _():
+            for src in srcs:
+                forward(src)
+
     def relay(src):
         to_y(src).wait_recv()
         y_to_sib(src).start()
@@ -240,6 +246,21 @@
             res[to] = out
             return_to(to).start()
 
+    def give_back_when(condition, srcs):
+        @pl.when(condition)
+        def _():
+            for at in srcs:
+                give_back(at)
+
+    def y_go_ordered(a, b):
+        @pl.when(upper == 1)
+        def _():
+            y_go(a + b)
+
+        @pl.when(upper == 0)
+        def _():
+            y_go(b + a)
+
     across = flip(me, 1)
     level, side = me // 2, me % 2
     levels = n_ep // 2
@@ -279,6 +300,11 @@
         return remote(at, at, k2_send.at[b], kv_recv.at[b, level], (lax.rem(me + 4, n_ep), tp))
 
     def kv_first():
+        @pl.when(level < levels - 1)
+        def _():
+            for b in range(2):
+                kv_copy(b, level).start()
+
         @pl.when(level == pinch - 1)
         def _():
             for b in range(4):
@@ -286,7 +312,7 @@
 
         @pl.when(level < levels - 1)
         def _():
-            for b in range(4):
+            for b in range(2, 4):
                 kv_copy(b, level).start()
 
     def kv_hop(step):
@@ -369,6 +395,8 @@
         def _():
             attend(level - step)
 
+    top_level = level == levels - 1
+
     def att_swap():
         return remote(mix.at[other], att.at[side], x_send.at[3], x_recv.at[3], (across, tp))
 
@@ -380,6 +408,11 @@
         att_swap().start()
         att[side] = mix[side]
 
+    def normalise_when(condition):
+        @pl.when(condition)
+        def _():
+            normalise()
+
     def h_pair(y):
         return remote(
             hp.at[flip(tp, 2 * y + 1)], hsib.at[y], h_send.at[y], h_recv.at[y], (me, sib_tp)
@@ -395,18 +428,28 @@
         h_pair(1).start()
         h_pair(0).start()
 
+    def project_when(condition):
+        @pl.when(condition)
+        def _():
+            project()
+
+    def h_send_over_when(condition):
+        @pl.when(condition)
+        def _():
+            h_send_over()
+
     def h_send_over():
         h_pair(1).wait_recv()
         hysend[...] = (hp[y_tp].astype(F32) + hsib[1].astype(F32)).astype(BF16)
         h_over().start()
 
     def drain():
-        for src in others(near) + sources(inner) + sources(outer):
+        for src in others(near) + sources(early) + sources(late):
             to_sib(src).wait_send()
             to_y(src).wait_send()
             y_to_sib(src).wait_send()
             return_to(src).wait_send()
-        for src in sources(near) + sources(inner) + sources(outer):
+        for src in sources(near) + sources(early) + sources(late):
             over_y(src).wait_send()
         for at in others(near):
             dispatch_to(at).wait_send()
@@ -430,7 +473,7 @@
         ).astype(BF16)
 
     def combine():
-        for src in others(near) + sources(inner) + sources(outer):
+        for src in others(near) + sources(early) + sources(late):
             return_from(src).wait_recv()
         got = ret[...].reshape(slots, cols)
         expert[...] = (dot(high[...], got) + dot(low[...], got)).astype(BF16)
@@ -439,8 +482,8 @@
     send_mate()
     own_rows()
     weigh()
+    swap_start()
     forward(others(near)[0])
-    swap_start()
     forward(others(near)[1])
     for at in others(near)[2:]: forward(at)
     expand(at_middle)
@@ -449,77 +492,78 @@
     expand(~at_middle)
     kv_first()
     for at in others(near)[1:]: relay(at)
-    for at in sources(inner)[:1]: forward(at)
+    attend_own()
     for copy in weights[:2]: copy.wait()
-    for at in sources(inner)[1:]: forward(at)
     for at in others(near): arrived(at)
     gate_up(near, 0, 4)
-    for at in sources(outer)[:1]: forward(at)
-    for at in sources(inner)[:1]: relay(at)
+    for at in sources(early): forward(at)
     gate_up(near, 4, 7)
-    for at in sources(outer)[1:]: forward(at)
-    for at in sources(inner)[1:]: relay(at)
+    for at in sources(late)[:1]: forward(at)
+    for at in sources(early)[:1]: relay(at)
+    hop_upper(1, 2)
     weights[2].wait()
     for r in (3, 1): down(near, r)
     pair(near, 0, 1)
     pair(near, 0, 0)
+    for at in sources(late)[1:]: forward(at)
+    for at in sources(early)[1:]: relay(at)
     for r in (2, 0): down(near, r)
-    for at in sources(inner): arrived(at)
-    gate_up(inner, 0, 7)
-    for at in sources(outer)[:1]: relay(at)
+    y_sum(near, 0)
+    y_go(sources(near)[:half // 2])
+    for at in sources(early): arrived(at)
+    gate_up(early, 0, 7)
+    for at in sources(late)[:1]: relay(at)
     hop_lower()
-    down(inner, 3)
-    pair(inner, 1, 1)
-    down(inner, 2)
-    for at in sources(outer)[1:]: relay(at)
-    hop_upper(1, 2)
-    down(inner, 1)
-    pair(inner, 1, 0)
-    down(inner, 0)
-    y_sum(inner, 1)
-    y_go(sources(inner))
-    for at in sources(outer): arrived(at)
-    gate_up(outer, 0, 7)
+    down(early, 3)
+    pair(early, 1, 1)
+    down(early, 2)
+    for at in sources(late)[1:]: relay(at)
+    down(early, 1)
+    pair(early, 1, 0)
+    down(early, 0)
+    y_sum(early, 1)
+    y_go(sources(early))
+    for at in sources(late): arrived(at)
+    gate_up(late, 0, 7)
     hop_upper(2, levels)
-    down(outer, 3)
-    pair(outer, 2, 1)
-    down(outer, 2)
-    down(outer, 1)
-    pair(outer, 2, 0)
-    down(outer, 0)
-    y_sum(outer, 2)
-    y_go(sources(outer))
-    y_sum(near, 0)
-    y_go(sources(near))
-    attend_own()
+    down(late, 3)
+    pair(late, 2, 1)
+    down(late, 2)
+    down(late, 1)
+    pair(late, 2, 0)
+    down(late, 0)
+    y_sum(late, 2)
+    y_go(sources(late) + sources(near)[half // 2:])
+    pairs[0, 0].wait_recv()
     pairs[1, 0].wait_recv()
-    for at in sources(inner): give_back(at)
+    for i, at in enumerate(sources(near)[:half // 2]): give_back(at, i == 0)
+    for at in sources(early)[:quarter // 2]: give_back(at)
     kv_last(1)
     attend_at(1)
-    pairs[2, 0].wait_recv()
-    for at in sources(outer): give_back(at)
+    for at in sources(early)[quarter // 2:]: give_back(at)
     for step in range(2, levels): kv_last(step); attend_at(step)
     normalise()
-    pairs[0, 0].wait_recv()
-    for i, at in enumerate(sources(near)): give_back(at, i == 0)
     weights[3].wait()
-    project()
-    h_send_over()
+    project_when(upper == 0)
+    pairs[2, 0].wait_recv()
+    for at in sources(late): give_back(at)
+    h_send_over_when(upper == 0)
+    for at in sources(near)[half // 2:]: give_back(at)
+    project_when(upper == 1)
+    h_send_over_when(upper == 1)
     combine()
     drain()
     mix_out()
 
 
-def settle(mixer_in, expert_in, mixer, expert, a, b, load, store):
-    pairs = ((mixer_in, a, mixer), (expert_in, b, expert))
-    loads = [pltpu.make_async_copy(x, y, load.at[i]) for i, (x, y, _) in enumerate(pairs)]
-    stores = [pltpu.make_async_copy(y, z, store.at[i]) for i, (_, y, z) in enumerate(pairs)]
-    for copy in loads:
+def settle(mixer_in, expert_in, mixer, expert, store):
+    copies = [
+        pltpu.make_async_copy(a, b, store.at[i])
+        for i, (a, b) in enumerate(((mixer_in, mixer), (expert_in, expert)))
+    ]
+    for copy in copies:
         copy.start()
-    for i in range(2):
-        loads[i].wait()
-        stores[i].start()
-    for copy in stores:
+    for copy in copies:
         copy.wait()
 
 
@@ -545,8 +589,8 @@
             functools.partial(kernel, n_ep, cap),
             name="both_halves",
             out_shape=(
-                jax.ShapeDtypeStruct((q_rows // 4, width), BF16),
-                jax.ShapeDtypeStruct((tokens, cols), BF16),
+                pltpu.VMEM((q_rows // 4, width), BF16),
+                pltpu.VMEM((tokens, cols), BF16),
             ),
             in_specs=[pl.BlockSpec(memory_space=pltpu.SMEM)] + [vm] * 8 + [hbm] * 4,
             out_specs=(vm, vm),
@@ -606,10 +650,10 @@
             settle,
             name="settle",
             out_shape=tuple(jax.ShapeDtypeStruct(o.shape, o.dtype) for o in outs),
-            in_specs=[hbm] * 2,
+            in_specs=[vm] * 2,
             out_specs=(hbm, hbm),
-            scratch_shapes=[pltpu.VMEM(o.shape, o.dtype) for o in outs] + [dma((2,)), dma((2,))],
-        )(*outs)
+            scratch_shapes=[dma((2,))],
+        )(*[pltpu.with_memory_space_constraint(o, pltpu.VMEM) for o in outs])
 
     placed = (
         P("ep", "tp"), P("ep", "tp"), P("ep", "tp"), P("tp"), P(), P("tp", None), P("ep", None), P(),

time: 62 us -> 55.6 us (0.90)
  the two profiles are of different devices: /device:TPU:0 before, /device:TPU:27 now
where the time goes in v2:
time: 55.6 us; the launch traced here: 55.5 us
  Pallas kernels  54.7 us (98%)
  between operations  0.8 us (1%)
    pallas_call x1, Pallas kernels, shards(): pl.pallas_call(functools.partial(kernel, n_ep, cap), name='both_halves',...  53.9 us

profile of v2, /device:TPU:27, one launch (start us, length us, event | category | flops | bytes accessed | tf_op | source)
XLA Modules:
  0.0 55.5 jit_solution(8660357697007552121)
XLA Ops:
  0.6 53.9 %both_halves.1 = (bf16[64,2048]{1,0:T(8,128)(2,1)S(1)}, bf16[192,512]{1,0:T(8,128)(2,1)S(1)}) custom-call(f32[2]{0:T(128)} %lam.1, bf16[256,256]{1,0:T(8,128)(2,1)} %q.1, bf16[256,256]{1,0:T(8,128)(2,1)} %k.1, bf16[256,256]{1,0:T(8,128)(2,1)} %v.1, f32[1,128]{1,0:T(1,128)} %bitcast.13, bf16[192,2048]{1,0:T(8,128)(2,1)} %x.1, f32[1,2048]{1,0:T(1,128)} %bitcast.10, ...), custom_call_target="tpu_custom_call" | custom-call | tf_op jit(solution)/shard_map/both_halves/pallas_call | solution.py:588
  54.5 0.8 %settle.1 = (bf16[64,2048]{1,0:T(8,128)(2,1)}, bf16[192,512]{1,0:T(8,128)(2,1)}) custom-call(bf16[64,2048]{1,0:T(8,128)(2,1)S(1)} %get-tuple-element.4.mixer_in, bf16[192,512]{1,0:T(8,128)(2,1)S(1)} %get-tuple-element.5.expert_in), custom_call_target="tpu_custom_call" | custom-call | tf_op jit(solution)/shard_map/settle/pallas_call | solution.py:649

commit v3 on v2

--- a/solution.py
+++ b/solution.py
@@ -38,7 +38,9 @@
     tp = lax.axis_index("tp")
     half, quarter = n_ep // 2, n_ep // 4
     upper = me // half
-    near = (upper * half, half)
+    side_base = me // quarter * quarter
+    near = (side_base, quarter)
+    facing = (upper * n_ep + quarter - side_base, quarter)
     early = ((1 - upper) * half, quarter)
     late = ((1 - upper) * half + quarter, quarter)
     mate = flip(me, half + quarter)
@@ -110,8 +112,8 @@
         base, size = group
         return [flip(base + me % size, i) for i in range(size)]
 
-    def others(group):
-        return sources(group)[1:] if group is near else sources(group)
+    beside = sources(near)[1:]
+    mates = beside + sources(facing)
 
     def send(ds):
         for d in ds:
@@ -131,7 +133,7 @@
             place = here.astype(F32)
             pick = ((place == info_in[0:1]) | (place == info_in[1:2])).astype(F32).astype(BF16)
             spread[...] = dot(pick, nrm_in[...]).astype(BF16).reshape(half, cap, cols)
-            for at in others(near):
+            for at in mates:
                 spread_to(at).start()
             arr[tp, mate] = spread[me - first]
 
@@ -179,6 +181,12 @@
         def _():
             for src in srcs:
                 forward(src)
+
+    def relay_when(condition, srcs):
+        @pl.when(condition)
+        def _():
+            for src in srcs:
+                relay(src)
 
     def relay(src):
         to_y(src).wait_recv()
@@ -302,18 +310,13 @@
     def kv_first():
         @pl.when(level < levels - 1)
         def _():
-            for b in range(2):
+            for b in range(4):
                 kv_copy(b, level).start()
 
         @pl.when(level == pinch - 1)
         def _():
             for b in range(4):
                 kv_skip(b).start()
-
-        @pl.when(level < levels - 1)
-        def _():
-            for b in range(2, 4):
-                kv_copy(b, level).start()
 
     def kv_hop(step):
         for b in range(4):
@@ -397,6 +400,11 @@
 
     top_level = level == levels - 1
 
+    def attend_when(condition, step):
+        @pl.when(condition & (level >= step))
+        def _():
+            attend(level - step)
+
     def att_swap():
         return remote(mix.at[other], att.at[side], x_send.at[3], x_recv.at[3], (across, tp))
 
@@ -444,14 +452,14 @@
         h_over().start()
 
     def drain():
-        for src in others(near) + sources(early) + sources(late):
+        for src in mates + sources(early) + sources(late):
             to_sib(src).wait_send()
             to_y(src).wait_send()
             y_to_sib(src).wait_send()
             return_to(src).wait_send()
-        for src in sources(near) + sources(early) + sources(late):
+        for src in sources(near) + sources(facing) + sources(early) + sources(late):
             over_y(src).wait_send()
-        for at in others(near):
+        for at in mates:
             dispatch_to(at).wait_send()
             spread_to(at).wait_send()
         for i in range(2):
@@ -473,51 +481,64 @@
         ).astype(BF16)
 
     def combine():
-        for src in others(near) + sources(early) + sources(late):
+        for src in mates + sources(early) + sources(late):
             return_from(src).wait_recv()
         got = ret[...].reshape(slots, cols)
         expert[...] = (dot(high[...], got) + dot(low[...], got)).astype(BF16)
 
-    send(range(1, half))
+    send(range(1, quarter))
     send_mate()
+    send(range(quarter, half))
     own_rows()
     weigh()
     swap_start()
-    forward(others(near)[0])
-    forward(others(near)[1])
-    for at in others(near)[2:]: forward(at)
+    for at in beside: forward(at)
+    expand(~at_middle)
+    for at in beside: relay(at)
     expand(at_middle)
-    relay(others(near)[0])
     swap_wait()
-    expand(~at_middle)
     kv_first()
-    for at in others(near)[1:]: relay(at)
+    for at in sources(facing): forward(at)
+    for copy in weights[:2]: copy.wait()
+    for at in beside: arrived(at)
+    gate_up(near, 0, 7)
+    weights[2].wait()
+    down(near, 3)
+    pair(near, 0, 1)
+    down(near, 1)
+    pair(near, 0, 0)
+    down(near, 2)
+    down(near, 0)
+    for at in sources(facing): relay(at)
+    for at in sources(early): forward(at)
+    for at in sources(late)[:quarter // 2]: forward(at)
+    for at in sources(facing): arrived(at)
+    gate_up(facing, 0, 7)
+    for at in sources(late)[quarter // 2:]: forward(at)
+    down(facing, 3)
+    pair(facing, 3, 1)
+    down(facing, 1)
+    pair(facing, 3, 0)
+    down(facing, 2)
+    down(facing, 0)
+    hop_upper(1, 2)
+    for at in sources(early)[:quarter // 2]: relay(at)
     attend_own()
-    for copy in weights[:2]: copy.wait()
-    for at in others(near): arrived(at)
-    gate_up(near, 0, 4)
-    for at in sources(early): forward(at)
-    gate_up(near, 4, 7)
-    for at in sources(late)[:1]: forward(at)
-    for at in sources(early)[:1]: relay(at)
-    hop_upper(1, 2)
-    weights[2].wait()
-    for r in (3, 1): down(near, r)
-    pair(near, 0, 1)
-    pair(near, 0, 0)
-    for at in sources(late)[1:]: forward(at)
-    for at in sources(early)[1:]: relay(at)
-    for r in (2, 0): down(near, r)
+    for at in sources(early)[quarter // 2:]: relay(at)
+    kv_last(1)
+    attend_when(level <= 1, 1)
+    normalise_when(level <= 1)
     y_sum(near, 0)
-    y_go(sources(near)[:half // 2])
+    y_go(sources(near))
     for at in sources(early): arrived(at)
     gate_up(early, 0, 7)
-    for at in sources(late)[:1]: relay(at)
+    for at in sources(late)[:quarter // 2]: relay(at)
     hop_lower()
     down(early, 3)
     pair(early, 1, 1)
     down(early, 2)
-    for at in sources(late)[1:]: relay(at)
+    for at in sources(late)[quarter // 2:]: relay(at)
+    hop_upper(2, levels)
     down(early, 1)
     pair(early, 1, 0)
     down(early, 0)
@@ -525,7 +546,6 @@
     y_go(sources(early))
     for at in sources(late): arrived(at)
     gate_up(late, 0, 7)
-    hop_upper(2, levels)
     down(late, 3)
     pair(late, 2, 1)
     down(late, 2)
@@ -533,24 +553,27 @@
     pair(late, 2, 0)
     down(late, 0)
     y_sum(late, 2)
-    y_go(sources(late) + sources(near)[half // 2:])
+    y_go(sources(late))
+    y_sum(facing, 3)
+    y_go(sources(facing))
     pairs[0, 0].wait_recv()
     pairs[1, 0].wait_recv()
-    for i, at in enumerate(sources(near)[:half // 2]): give_back(at, i == 0)
+    for i, at in enumerate(sources(near)): give_back(at, i == 0)
+    weights[3].wait()
     for at in sources(early)[:quarter // 2]: give_back(at)
-    kv_last(1)
-    attend_at(1)
+    project_when(level <= 1)
+    attend_when(level > 1, 1)
     for at in sources(early)[quarter // 2:]: give_back(at)
     for step in range(2, levels): kv_last(step); attend_at(step)
-    normalise()
-    weights[3].wait()
-    project_when(upper == 0)
+    normalise_when(level > 1)
+    h_send_over_when(level <= 1)
     pairs[2, 0].wait_recv()
+    pairs[3, 0].wait_recv()
     for at in sources(late): give_back(at)
-    h_send_over_when(upper == 0)
-    for at in sources(near)[half // 2:]: give_back(at)
-    project_when(upper == 1)
-    h_send_over_when(upper == 1)
+    project_when(level > 1)
+    for at in sources(facing)[:quarter // 2]: give_back(at)
+    h_send_over_when(level > 1)
+    for at in sources(facing)[quarter // 2:]: give_back(at)
     combine()
     drain()
     mix_out()
@@ -631,7 +654,7 @@
                 dma((n_ep,)), dma((n_ep,)),
                 dma((3, n_ep)), dma((3, n_ep)),
                 dma((n_ep,)), dma((n_ep,)),
-                dma((3, 2)), dma((3, 2)),
+                dma((4, 2)), dma((4, 2)),
                 dma((n_ep,)), dma((n_ep,)),
                 dma((2,)),dma((2,)),
                 dma((4,)), dma((4,)),

time: 55.6 us -> 54.3 us (0.977)
  the two profiles are of different devices: /device:TPU:27 before, /device:TPU:0 now
where the time goes in v3:
time: 54.3 us; the launch traced here: 54.2 us
  Pallas kernels  53.4 us (98%)
  between operations  0.8 us (1%)
    pallas_call x1, Pallas kernels, shards(): pl.pallas_call(functools.partial(kernel, n_ep, cap), name='both_halves',...  52.6 us

profile of v3, /device:TPU:0, one launch (start us, length us, event | category | flops | bytes accessed | tf_op | source)
XLA Modules:
  0.0 54.2 jit_solution(13029099877053732951)
XLA Ops:
  0.6 52.6 %both_halves.1 = (bf16[64,2048]{1,0:T(8,128)(2,1)S(1)}, bf16[192,512]{1,0:T(8,128)(2,1)S(1)}) custom-call(f32[2]{0:T(128)} %lam.1, bf16[256,256]{1,0:T(8,128)(2,1)} %q.1, bf16[256,256]{1,0:T(8,128)(2,1)} %k.1, bf16[256,256]{1,0:T(8,128)(2,1)} %v.1, f32[1,128]{1,0:T(1,128)} %bitcast.13, bf16[192,2048]{1,0:T(8,128)(2,1)} %x.1, f32[1,2048]{1,0:T(1,128)} %bitcast.10, ...), custom_call_target="tpu_custom_call" | custom-call | tf_op jit(solution)/shard_map/both_halves/pallas_call | solution.py:611
  53.3 0.8 %settle.1 = (bf16[64,2048]{1,0:T(8,128)(2,1)}, bf16[192,512]{1,0:T(8,128)(2,1)}) custom-call(bf16[64,2048]{1,0:T(8,128)(2,1)S(1)} %get-tuple-element.4.mixer_in, bf16[192,512]{1,0:T(8,128)(2,1)S(1)} %get-tuple-element.5.expert_in), custom_call_target="tpu_custom_call" | custom-call | tf_op jit(solution)/shard_map/settle/pallas_call | solution.py:672

commit v4 on v3

--- a/solution.py
+++ b/solution.py
@@ -298,28 +298,28 @@
             swap(i).wait_recv()
 
     def kv_copy(b, lev):
-        buf = kbuf if b < 2 else vbuf
-        at = buf.at[lev, b % 2]
+        buf = vbuf if b else kbuf
+        at = buf.at[lev]
         return remote(at, at, kv_send.at[b, lev], kv_recv.at[b, lev], (lax.rem(me + 2, n_ep), tp))
 
     def kv_skip(b):
-        buf = kbuf if b < 2 else vbuf
-        at = buf.at[level, b % 2]
+        buf = vbuf if b else kbuf
+        at = buf.at[level]
         return remote(at, at, k2_send.at[b], kv_recv.at[b, level], (lax.rem(me + 4, n_ep), tp))
 
     def kv_first():
         @pl.when(level < levels - 1)
         def _():
-            for b in range(4):
+            for b in range(2):
                 kv_copy(b, level).start()
 
         @pl.when(level == pinch - 1)
         def _():
-            for b in range(4):
+            for b in range(2):
                 kv_skip(b).start()
 
     def kv_hop(step):
-        for b in range(4):
+        for b in range(2):
             kv_copy(b, level - step).wait_recv()
             kv_copy(b, level - step).start()
 
@@ -338,12 +338,12 @@
     def kv_last(step):
         @pl.when(((level == levels - 1) & (level >= step)) | ((level == pinch) & (step == 1)))
         def _():
-            for b in range(4):
+            for b in range(2):
                 kv_copy(b, level - step).wait_recv()
 
     def kv_finish():
         def step(lev, carry):
-            for b in range(4):
+            for b in range(2):
                 kv_copy(b, lev).wait_send()
             return carry
 
@@ -358,7 +358,7 @@
 
         @pl.when(level == pinch - 1)
         def _():
-            for b in range(4):
+            for b in range(2):
                 kv_skip(b).wait_send()
 
     both = 2 * q_rows
@@ -658,7 +658,7 @@
                 dma((n_ep,)), dma((n_ep,)),
                 dma((2,)),dma((2,)),
                 dma((4,)), dma((4,)),
-                dma((4, half)), dma((4, half)), dma((4,)),
+                dma((2, half)), dma((2, half)), dma((2,)),
                 dma((3,)), dma((3,)),
             ],
             compiler_params=pltpu.CompilerParams(

time: 54.3 us -> 54.1 us (level)
  no operation moved by 1% of the time
where the time goes in v4:
time: 54.1 us; the launch traced here: 53.9 us
  Pallas kernels  53.1 us (98%)
  between operations  0.8 us (1%)
    pallas_call x1, Pallas kernels, shards(): pl.pallas_call(functools.partial(kernel, n_ep, cap), name='both_halves',...  52.3 us

profile of v4, /device:TPU:0, one launch (start us, length us, event | category | flops | bytes accessed | tf_op | source)
XLA Modules:
  0.0 53.9 jit_solution(18113395367371828394)
XLA Ops:
  0.6 52.3 %both_halves.1 = (bf16[64,2048]{1,0:T(8,128)(2,1)S(1)}, bf16[192,512]{1,0:T(8,128)(2,1)S(1)}) custom-call(f32[2]{0:T(128)} %lam.1, bf16[256,256]{1,0:T(8,128)(2,1)} %q.1, bf16[256,256]{1,0:T(8,128)(2,1)} %k.1, bf16[256,256]{1,0:T(8,128)(2,1)} %v.1, f32[1,128]{1,0:T(1,128)} %bitcast.13, bf16[192,2048]{1,0:T(8,128)(2,1)} %x.1, f32[1,2048]{1,0:T(1,128)} %bitcast.10, ...), custom_call_target="tpu_custom_call" | custom-call | tf_op jit(solution)/shard_map/both_halves/pallas_call | solution.py:611
  53.0 0.8 %settle.1 = (bf16[64,2048]{1,0:T(8,128)(2,1)}, bf16[192,512]{1,0:T(8,128)(2,1)}) custom-call(bf16[64,2048]{1,0:T(8,128)(2,1)S(1)} %get-tuple-element.4.mixer_in, bf16[192,512]{1,0:T(8,128)(2,1)S(1)} %get-tuple-element.5.expert_in), custom_call_target="tpu_custom_call" | custom-call | tf_op jit(solution)/shard_map/settle/pallas_call | solution.py:672
